TPU v7x, 32 devices: a whole 2x2x4 slice. The times are simulated.
32 devices in a mesh: sp: 8 (over z, x), tp: 4 (over y, core).
Axes of the slice: x: 2, y: 2, z: 4, core: 2. Of those that a mesh axis runs over, the one named last changes fastest.
Arguments:
- target: bfloat16 [1024, 4096], P('sp', 'tp'), may hold values from -300 to 300
- gain: float32 [4096], P('tp'), may hold values from 0.1 to 1.9
- w_query: bfloat16 [4096, 4096], P('tp'), may hold values from -0.09375 to 0.09375
- queries: bfloat16 [1024, 4096], P('sp', 'tp'), may hold values from -13 to 13
- keys: bfloat16 [4096, 1024], P('sp'), may hold values from -4 to 4
- values: bfloat16 [4096, 1024], P('sp'), may hold values from -4 to 4
- attn_out: bfloat16 [1024, 4096], P('sp', 'tp'), may hold values from -4 to 4
- grad_out: bfloat16 [1024, 4096], P('sp', 'tp'), may hold values from -64 to 64
Outputs:
- grad_rows: bfloat16 [1024, 4096], P('sp', 'tp')
- grad_weight: float32 [4096, 4096], P(('tp', 'sp'))
- grad_keys: float32 [4096, 1024], P(('sp', 'tp'))
- grad_values: float32 [4096, 1024], P(('sp', 'tp'))
All inputs are finite; a program needn't handle non-finite values.
Results may differ from a plain program's by a relative error of at most 0.018.
Values may be sent and summed in bfloat16 or wider, within the bound.
A program may use at most 64 MiB of HBM per device.

v0:
```python
import math
import jax
import jax.numpy as jnp
from jax import lax
from jax.sharding import PartitionSpec as P

WIDTH = 4096
HEADS = 16
KV_HEADS = 4
HEAD_DIM = 256
norm_eps = 1e-06


def merged(part, axis, combine):
    gathered = jax.tree.map(lambda a: lax.all_gather(a, axis), part)

    def take(source):
        return jax.tree.map(lambda a: lax.dynamic_index_in_dim(a, source, 0, False), gathered)

    return lax.fori_loop(
        1, lax.axis_size(axis), lambda source, state: combine(state, take(source)), take(0)
    )


def join_stats(first_part, second_part):
    row_peak = jnp.maximum(first_part[0], second_part[0])
    summed = first_part[1] * jnp.exp(first_part[0] - row_peak) + second_part[1] * jnp.exp(
        second_part[0] - row_peak
    )
    return (row_peak, summed, first_part[2] + second_part[2])


def local(target, gain, w_query, queries, keys, values, attn_out, grad_out):
    local_heads = queries.shape[1] // HEAD_DIM
    group_size = HEADS // KV_HEADS
    score_scale = HEAD_DIM ** (-0.5)
    own_rows = queries.shape[0]
    src_rows = keys.shape[0]
    kv_index = lax.axis_index("tp") * local_heads // group_size
    key_own = lax.dynamic_slice_in_dim(keys, kv_index * HEAD_DIM, HEAD_DIM, 1)
    value_own = lax.dynamic_slice_in_dim(values, kv_index * HEAD_DIM, HEAD_DIM, 1)
    out_heads = attn_out.reshape(own_rows, local_heads, HEAD_DIM).astype(jnp.float32)
    grad_heads = grad_out.reshape(own_rows, local_heads, HEAD_DIM).astype(jnp.float32)
    delta_own = jnp.sum(out_heads * grad_heads, axis=2)
    empty_sum = jnp.zeros((src_rows, HEAD_DIM), jnp.float32)
    total_rows = own_rows * lax.axis_size("sp")
    position = lax.axis_index("sp") * own_rows
    delta_full = lax.dynamic_update_slice_in_dim(
        jnp.zeros((total_rows, local_heads), jnp.float32), delta_own, position, 0
    )
    query_all, grad_all = (
        lax.all_gather(queries, "sp", axis=0, tiled=True),
        lax.all_gather(grad_out, "sp", axis=0, tiled=True),
    )
    block_rows = math.gcd(total_rows, 512)
    block_count = total_rows // block_rows
    query_blocks = query_all.reshape(block_count, block_rows, local_heads, HEAD_DIM)
    grad_blocks = grad_all.reshape(block_count, block_rows, local_heads, HEAD_DIM)

    def block_stats(query_block):
        scores = (
            jnp.einsum("qhd,sd->hqs", query_block, key_own, preferred_element_type=jnp.float32)
            * score_scale
        )
        row_peak = jnp.max(scores, axis=2)
        row_total = jnp.sum(jnp.exp(scores - row_peak[:, :, None]), axis=2)
        return (row_peak, row_total)

    peaks, totals = lax.map(block_stats, query_blocks)
    peaks, totals, delta_full = merged((peaks, totals, delta_full), "sp", join_stats)
    log_totals = peaks + jnp.log(totals)
    delta_blocks = delta_full.reshape(block_count, block_rows, local_heads)

    def block_grads(running, inputs):
        query_block, grad_block, delta_block, log_block = inputs
        scores = (
            jnp.einsum("qhd,sd->hqs", query_block, key_own, preferred_element_type=jnp.float32)
            * score_scale
        )
        weights = jnp.exp(scores - log_block[:, :, None])
        grad_weights = jnp.einsum(
            "qhd,sd->hqs", grad_block, value_own, preferred_element_type=jnp.float32
        )
        delta_cols = jnp.transpose(delta_block)
        grad_scores = (weights * (grad_weights - delta_cols[:, :, None]) * score_scale).astype(
            jnp.bfloat16
        )
        key_sum = running[0] + jnp.einsum(
            "hqs,qhd->sd", grad_scores, query_block, preferred_element_type=jnp.float32
        )
        value_sum = running[1] + jnp.einsum(
            "hqs,qhd->sd",
            weights.astype(jnp.bfloat16),
            grad_block,
            preferred_element_type=jnp.float32,
        )
        query_part = jnp.einsum(
            "hqs,sd->qhd", grad_scores, key_own, preferred_element_type=jnp.float32
        )
        return ((key_sum, value_sum), query_part)

    (key_sum, value_sum), query_parts = lax.scan(
        block_grads, (empty_sum, empty_sum), (query_blocks, grad_blocks, delta_blocks, log_totals)
    )
    query_parts = query_parts.reshape(total_rows, 1, local_heads * HEAD_DIM)
    received = lax.all_to_all(
        query_parts.astype(jnp.bfloat16), "sp", split_axis=0, concat_axis=1, tiled=True
    ).astype(query_parts.dtype)
    query_grad = jnp.sum(received, axis=1)
    key_cols = key_sum.reshape(src_rows, 1, HEAD_DIM)
    value_cols = value_sum.reshape(src_rows, 1, HEAD_DIM)
    key_parts, value_parts = (
        lax.all_to_all(
            key_cols.astype(jnp.bfloat16), "tp", split_axis=0, concat_axis=1, tiled=True
        ).astype(key_cols.dtype),
        lax.all_to_all(
            value_cols.astype(jnp.bfloat16), "tp", split_axis=0, concat_axis=1, tiled=True
        ).astype(value_cols.dtype),
    )
    part_rows = key_parts.shape[0]
    per_kv = key_parts.shape[1] // KV_HEADS
    grad_keys = (
        key_parts.reshape(part_rows, KV_HEADS, per_kv, HEAD_DIM)
        .sum(axis=2)
        .reshape(part_rows, KV_HEADS * HEAD_DIM)
    )
    grad_values = (
        value_parts.reshape(part_rows, KV_HEADS, per_kv, HEAD_DIM)
        .sum(axis=2)
        .reshape(part_rows, KV_HEADS * HEAD_DIM)
    )
    query_grad = query_grad.astype(jnp.bfloat16)
    query_all_heads = lax.all_gather(query_grad, "tp", axis=1, tiled=True)
    grad_rows = lax.dot_general(
        query_all_heads, w_query, (((1,), (1,)), ((), ())), preferred_element_type=jnp.float32
    ).astype(jnp.bfloat16)
    target_wide = target.astype(jnp.float32)
    squares = lax.psum(jnp.sum(target_wide * target_wide, axis=1), "tp")
    inverse = lax.rsqrt(squares / WIDTH + norm_eps)
    normed = (target_wide * inverse[:, None] * gain).astype(jnp.bfloat16)
    grad_weight = lax.psum_scatter(
        lax.dot_general(
            normed, query_all_heads, (((0,), (0,)), ((), ())), preferred_element_type=jnp.float32
        ).astype(jnp.bfloat16),
        "sp",
        scatter_dimension=0,
        tiled=True,
    ).astype(jnp.float32)
    return (grad_rows, grad_weight, grad_keys, grad_values)


def solution(mesh):
    return jax.shard_map(
        local,
        mesh=mesh,
        in_specs=(
            P("sp", "tp"),
            P("tp"),
            P("tp", None),
            P("sp", "tp"),
            P("sp", None),
            P("sp", None),
            P("sp", "tp"),
            P("sp", "tp"),
        ),
        out_specs=(
            P("sp", "tp"),
            P(("tp", "sp"), None),
            P(("sp", "tp"), None),
            P(("sp", "tp"), None),
        ),
        check_vma=False,
    )
```

profile of v0, /device:TPU:0, one launch (start us, length us, event | category | flops | bytes accessed | tf_op | source)
XLA Modules:
  0.0 421.2 jit_solution(14617625495296849069)
XLA Ops:
  8.8 1.1 convert_multiply_fusion.2
  10.4 32.5 %all_gather.33 = f32[8,1024,4]{1,2,0:T(4,128)S(1)} all-gather(f32[1,1024,4]{1,2,0:T(4,128)S(1)} %constant_dynamic-update-slice_fusion), channel_id=1, replica_groups=mesh['sp'=8,'tp'=4] {'sp'}, dimensions={0}, use_global_device_ids=true | all-gather | bytes 147456 | tf_op jit(solution)/shard_map/all_gather | solution.py:15
  43.6 1.8 constant_dynamic-slice_fusion.1
  45.4 17.0 %all-gather.6.cloned.1.call-done = bf16[1024,1024]{1,0:T(8,128)(2,1)} async-done(((bf16[128,1024]{1,0:T(8,128)(2,1)}), bf16[1024,1024]{1,0:T(8,128)(2,1)}) %all-gather.6.cloned.1.call-update) | async-done | bytes 2097168 | tf_op jit(solution)/shard_map/all_gather | solution.py:52
  62.4 4.5 %reshape.71 = bf16[2,512,4,256]{3,2,1,0:T(4,128)(2,1)} reshape(bf16[1024,1024]{1,0:T(8,128)(2,1)} %all-gather.6.cloned.1.call-done) | data formatting | bytes 4194304 | tf_op jit(solution)/shard_map/reshape | solution.py:57
  66.9 1.9 copy.38
  68.7 3.0 while.46
  68.8 0.8 bitcast_reduce_fusion.2
  70.3 0.8 bitcast_reduce_fusion.2
  71.8 31.3 %all-gather.1 = f32[16,4,512]{2,1,0:T(4,128)S(1)} all-gather(f32[2,4,512]{2,1,0:T(4,128)S(1)} %get-tuple-element.265), channel_id=3, replica_groups=mesh['sp'=8,'tp'=4] {'sp'}, dimensions={0}, use_global_device_ids=true | all-gather | bytes 147456 | tf_op jit(solution)/shard_map/all_gather | solution.py:15
  103.1 30.8 %all-gather = f32[16,4,512]{2,1,0:T(4,128)S(1)} all-gather(f32[2,4,512]{2,1,0:T(4,128)S(1)} %get-tuple-element.264), channel_id=2, replica_groups=mesh['sp'=8,'tp'=4] {'sp'}, dimensions={0}, use_global_device_ids=true | all-gather | bytes 147456 | tf_op jit(solution)/shard_map/all_gather | solution.py:15
  134.5 10.6 %while.47 = (s32[]{:T(128)}, f32[2,4,512]{2,1,0:T(4,128)S(1)}, f32[2,4,512]{2,1,0:T(4,128)S(1)}, f32[1024,4]{0,1:T(4,128)S(1)}, f32[8,2,4,512]{3,2,1,0:T(4,128)}...) while((s32[]{:T(128)}, f32[2,4,512]{2,1,0:T(4,128)S(1)}, ...), condition=%wide.region_6.7_spmd, body=%wide.region_5.6_spmd.sunk | while | flops 28677 | bytes 147599 | solution.py:20
  134.5 0.7 bitcast_add_fusion.2
  135.2 0.8 fusion.62
  136.0 0.7 bitcast_add_fusion.2
  136.8 0.8 fusion.62
  137.5 0.7 bitcast_add_fusion.2
  138.3 0.8 fusion.62
  139.1 0.7 bitcast_add_fusion.2
  139.8 0.8 fusion.62
  140.6 0.7 bitcast_add_fusion.2
  141.3 0.8 fusion.62
  142.1 0.7 bitcast_add_fusion.2
  142.8 0.8 fusion.62
  143.6 0.7 bitcast_add_fusion.2
  144.3 0.8 fusion.62
  145.2 4.5 %reshape.72 = bf16[2,512,4,256]{3,2,1,0:T(4,128)(2,1)} reshape(bf16[1024,1024]{1,0:T(8,128)(2,1)} %all-gather.8.cloned.1.call-done) | data formatting | bytes 4194304 | tf_op jit(solution)/shard_map/reshape | solution.py:58
  149.6 18.0 %while.48 = (s32[]{:T(128)}, f32[512,256]{1,0:T(8,128)S(1)}, f32[512,256]{1,0:T(8,128)S(1)}, bf16[2,512,4,256]{3,1,2,0:T(8,128)(2,1)}, bf16[2,512,4,256]{3,1,2,0...) while((s32[]{:T(128)}, f32[512,256]{1,0:T(8,128)S(1)}, ...), condition=%wide.region_8.9_spmd.clone, body=%wide.region_7.8_spmd.clone.sunk | while | flops 2694316032 | bytes 48029940 | solution.py:102
  149.7 1.6 constant_dynamic-slice_fusion.4
  151.2 0.7 fusion.71
  152.0 1.5 fusion.74
  153.5 1.5 fusion.72
  155.0 0.9 fusion.73
  157.4 1.3 copy-done.2
  158.7 1.6 constant_dynamic-slice_fusion.4
  160.3 0.7 fusion.71
  161.0 1.5 fusion.74
  162.5 1.5 fusion.72
  164.1 0.8 fusion.73
  166.4 1.3 copy-done.2
  167.7 3.2 copy.40
  170.9 6.3 %convert_element_type.92 = bf16[1024,1,1024]{2,1,0:T(2,128)(2,1)} reshape(bf16[2,512,4,256]{3,2,1,0:T(4,128)(2,1)S(1)} %copy.40) | data formatting | bytes 4194304 | tf_op jit(solution)/shard_map/convert_element_type | solution.py:107
  177.7 12.8 %reduce.4 = bf16[1024,1024]{1,0:T(8,128)(2,1)S(1)} reduce(bf16[1024,1,1024]{2,1,0:T(2,128)(2,1)} %convert_element_type.92, bf16[]{:T(256)} %broadcast.49), dimensions={1}, to_apply=%convert_element_type.92.reduce_sub_computation | reduce | bytes 4194306 | tf_op jit(solution)/shard_map/convert_element_type | solution.py:107
  190.5 3.8 reshape.99
  194.2 38.8 %all_to_all.30 = bf16[8,2,65536]{2,1,0:T(2,128)(2,1)S(1)} all-to-all(bf16[8,2,65536]{2,1,0:T(2,128)(2,1)} %reshape.99), channel_id=1, replica_groups=mesh['sp'=8,'tp'=4] {'sp'}, dimensions={0} | all-to-all | bytes 4194304 | tf_op jit(solution)/shard_map/all_to_all | solution.py:106
  233.0 4.3 %reshape.100 = bf16[1024,1,1024]{2,1,0:T(2,128)(2,1)} reshape(bf16[8,2,65536]{2,1,0:T(2,128)(2,1)S(1)} %all_to_all.30) | data formatting | bytes 4194304
  237.3 3.0 copy.49
  240.4 1.1 reduce_sum.48
  241.7 5.9 %psum.7 = f32[128]{0:T(128)S(1)} all-reduce(f32[128]{0:T(128)S(1)} %fusion.36), channel_id=1, replica_groups=mesh['sp'=8,'tp'=4] {'tp'}, use_global_device_ids=true, to_apply=%region_11.12 | all-reduce | flops 128 | bytes 1024 | tf_op jit(solution)/shard_map/psum | solution.py:138
  247.6 9.8 %all-gather.10.cloned.1.call-done = bf16[128,4096]{1,0:T(8,128)(2,1)} async-done(((bf16[128,1024]{1,0:T(8,128)(2,1)}), bf16[128,4096]{1,0:T(8,128)(2,1)}) %all-gather.10.cloned.1.call-update) | async-done | bytes 1048592 | tf_op jit(solution)/shard_map/all_gather | solution.py:133
  257.4 6.9 %convolution_convert_fusion = bf16[1024,4096]{1,0:T(8,128)(2,1)} fusion(bf16[128,4096]{1,0:T(8,128)(2,1)} %all-gather.10.cloned.1.call-done, bf16[128,1024]{1,0:T(8,128)(2,1)S(1)} %copy-done.3, f32[1024]{0:T(1024)S(1)} %copy-done.8, f32[128]{0:T(128)S(1)} %add_rsqrt_fusion), kind=kOutput, calls=%fused_computation.47 | convolution fusion | flops 1078460416 | bytes 9703936 | tf_op jit(solution)/shard_map/dot_general | solution.py:142
  264.3 0.8 reduce.5
  265.1 0.8 reshape.101
  265.9 3.4 all-to-all-start.1
  269.4 0.8 reduce.6
  270.2 0.8 reshape.103
  270.9 4.3 %all-to-all-done.1 = bf16[4,2,16384]{2,1,0:T(2,128)(2,1)S(1)} async-done(((bf16[4,2,16384]{2,1,0:T(2,128)(2,1)}), bf16[4,2,16384]{2,1,0:T(2,128)(2,1)S(1)}, u32[]{:S(2)}, u32[]{:S(2)}) %all-to-all-start.1) | async-done | bytes 262176 | tf_op jit(solution)/shard_map/all_to_all | solution.py:113
  275.3 3.4 all-to-all-start.2
  279.9 0.9 copy.50
  280.8 3.9 all-to-all-done.2
  285.8 0.9 copy.51
  286.7 7.0 %convolution_convert_fusion.1 = bf16[128,1024]{1,0:T(8,128)(2,1)} fusion(bf16[128,4096]{1,0:T(8,128)(2,1)S(1)} %copy-done, bf16[1024,4096]{1,0:T(8,128)(2,1)} %param.16), kind=kOutput, calls=%fused_computation.48 | convolution fusion | flops 1073872896 | bytes 9699328 | tf_op jit(solution)/shard_map/dot_general | solution.py:134
  293.8 118.1 %reduce-scatter.2.cloned.1.call-done = bf16[128,4096]{1,0:T(8,128)(2,1)} async-done(((bf16[1024,4096]{1,0:T(8,128)(2,1)}), bf16[128,4096]{1,0:T(8,128)(2,1)}) %reduce-scatter.2.cloned.1.call-update) | async-done | bytes 1048592 | tf_op jit(solution)/shard_map/reduce_scatter | solution.py:141
  411.9 2.8 convert_element_type.81
  (66 shorter events, 10.8 us)
Async XLA Ops:
  7.2 55.2 %all-gather.6.cloned.1.call-start = ((), (), s32[]{:S(2)}) async-start(), calls=%async_computation.4 | async-start | bytes 2359296 | tf_op jit(solution)/shard_map/all_gather | solution.py:52
  7.9 137.2 %all-gather.8.cloned.1.call-start = ((), (), s32[]{:S(2)}) async-start(), calls=%async_computation.5 | async-start | bytes 2359296 | tf_op jit(solution)/shard_map/all_gather | solution.py:53
  8.6 248.7 %all-gather.10.cloned.1.call-start = ((), (), s32[]{:S(2)}) async-start(), calls=%async_computation.6 | async-start | bytes 1310720 | tf_op jit(solution)/shard_map/all_gather | solution.py:133
  42.9 0.7 copy-start.4
  103.0 30.8 %copy-start.5 = (f32[16,4,512]{2,1,0:T(4,128)}, f32[16,4,512]{2,1,0:T(4,128)S(1)}, u32[]{:S(2)}) copy-start(f32[16,4,512]{2,1,0:T(4,128)S(1)} %all-gather.1) | copy-start | bytes 393220
  133.8 0.7 copy-start.6
  152.0 1.5 copy-start.7
  155.0 1.6 copy-start.1
  157.3 1.3 copy-start.2
  161.0 1.5 copy-start.7
  164.0 1.6 copy-start.1
  166.3 1.3 copy-start.2
  237.3 4.2 %copy-start.3 = (bf16[128,1024]{1,0:T(8,128)(2,1)S(1)}, bf16[128,1024]{1,0:T(8,128)(2,1)}, u32[]{:S(2)}) copy-start(bf16[128,1024]{1,0:T(8,128)(2,1)} %param.14) | copy-start | bytes 786436
  237.3 20.0 %copy-start.8 = (f32[1024]{0:T(1024)S(1)}, f32[1024]{0:T(1024)}, u32[]{:S(2)}) copy-start(f32[1024]{0:T(1024)} %param.15) | copy-start | bytes 12292
  241.5 170.4 %reduce-scatter.2.cloned.1.call-start = ((), (), s32[]{:S(2)}) async-start(), calls=%async_computation.7 | async-start | bytes 9437184 | tf_op jit(solution)/shard_map/reduce_scatter | solution.py:141
  265.9 9.4 %all-to-all-start.1 = ((bf16[4,2,16384]{2,1,0:T(2,128)(2,1)}), bf16[4,2,16384]{2,1,0:T(2,128)(2,1)S(1)}, u32[]{:S(2)}, u32[]{:S(2)}) async-start(bf16[4,2,16384]{2,1,0:T(2,128)(2,1)} %reshape.101), calls=%async_computation.2 | async-start | bytes 524288 | tf_op jit(solution)/shard_map/all_to_all | solution.py:113
  270.9 15.8 %copy-start = (bf16[128,4096]{1,0:T(8,128)(2,1)S(1)}, bf16[128,4096]{1,0:T(8,128)(2,1)}, u32[]{:S(2)}) copy-start(bf16[128,4096]{1,0:T(8,128)(2,1)} %all-gather.10.cloned.1.call-done) | copy-start | bytes 3145732
  275.3 9.4 %all-to-all-start.2 = ((bf16[4,2,16384]{2,1,0:T(2,128)(2,1)}), bf16[4,2,16384]{2,1,0:T(2,128)(2,1)S(1)}, u32[]{:S(2)}, u32[]{:S(2)}) async-start(bf16[4,2,16384]{2,1,0:T(2,128)(2,1)} %reshape.103), calls=%async_computation.3 | async-start | bytes 524288 | tf_op jit(solution)/shard_map/all_to_all | solution.py:116
Sparse Core Ops, SparseCore 0:
  10.1 52.2 all-gather.5
  64.5 49.3 all-gather.7
  241.6 15.6 all-gather.9
  264.4 147.4 reduce-scatter.1
where the time goes:
time: 424 us; the launch traced here: 421 us
  waiting for transfers between devices  155 us (37%)
  blocking collectives  139 us (33%)
  local copies, waits for them, and re-layouts  47.3 us (11%)
  other arithmetic  32.8 us (8%)
  matrix products  26 us (6%)
  between operations  14 us (3%)
  starting transfers between devices  6.97 us (2%)
    reduce_scatter x1, waiting for transfers between devices, local(): lax.psum_scatter(lax.dot_general(normed, query_all_heads, (((0,), (0,)),...  118 us
    all_gather x3, blocking collectives, merged(): gathered = jax.tree.map(lambda a: lax.all_gather(a, axis), part)  94.6 us
    all_to_all x1, blocking collectives, local(): lax.all_to_all(query_parts.astype(jnp.bfloat16), 'sp', split_axis=0, conc...  38.8 us
    unnamed x22, local copies, waits for them, and re-layouts  18.2 us
    all_gather x1, waiting for transfers between devices, local(): lax.all_gather(queries, 'sp', axis=0, tiled=True)  17 us
    convert_element_type x1, other arithmetic, local(): query_parts.astype(jnp.bfloat16)  12.8 us
    convert_element_type x3, local copies, waits for them, and re-layouts, local(): query_parts.astype(jnp.bfloat16)  10 us
    all_gather x1, waiting for transfers between devices, local(): query_all_heads = lax.all_gather(query_grad, 'tp', axis=1, tiled=True)  9.77 us
  transfers between devices with their start and end apart: 6, of which 5 were waited for; matrix products, arithmetic and copies ran while one was open for 9% of the time, Pallas kernels for 0%

commit v1 on v0

--- a/solution.py
+++ b/solution.py
@@ -103,8 +103,16 @@
         block_grads, (empty_sum, empty_sum), (query_blocks, grad_blocks, delta_blocks, log_totals)
     )
     query_parts = query_parts.reshape(total_rows, 1, local_heads * HEAD_DIM)
-    received = lax.all_to_all(
-        query_parts.astype(jnp.bfloat16), "sp", split_axis=0, concat_axis=1, tiled=True
+    received = jnp.concatenate(
+        lax.all_to_all(
+            jnp.stack(
+                jnp.split(query_parts.astype(jnp.bfloat16), lax.axis_size("sp"), axis=0), axis=0
+            ),
+            "sp",
+            0,
+            0,
+        ),
+        axis=1,
     ).astype(query_parts.dtype)
     query_grad = jnp.sum(received, axis=1)
     key_cols = key_sum.reshape(src_rows, 1, HEAD_DIM)

time: 424 us -> 397 us (0.936)
  other arithmetic: 32.8 us -> 20 us
  local copies, waits for them, and re-layouts: 47.3 us -> 34.6 us
    convert_element_type x1 -> x0, other arithmetic: 12.8 us -> none  [local(): query_parts.astype(jnp.bfloat16)]
    unnamed x22 -> x26, local copies, waits for them, and re-layouts: 18.2 us -> 7.17 us
    convert_element_type x3 -> x2, local copies, waits for them, and re-layouts: 10 us -> 7.78 us  [local(): query_parts.astype(jnp.bfloat16)]
  transfers between devices with their start and end apart: 6 -> 6, of which waited for: 5 -> 5; matrix products, arithmetic and copies ran while one was open for 9% -> 10% of each run, Pallas kernels for 0% -> 0%
where the time goes in v1:
time: 397 us; the launch traced here: 395 us
  waiting for transfers between devices  154 us (39%)
  blocking collectives  139 us (35%)
  local copies, waits for them, and re-layouts  34.6 us (9%)
  matrix products  26.1 us (7%)
  other arithmetic  20 us (5%)
  between operations  14.1 us (4%)
  starting transfers between devices  6.97 us (2%)
    reduce_scatter x1, waiting for transfers between devices, local(): lax.psum_scatter(lax.dot_general(normed, query_all_heads, (((0,), (0,)),...  118 us
    all_gather x3, blocking collectives, merged(): gathered = jax.tree.map(lambda a: lax.all_gather(a, axis), part)  94.4 us
    all_to_all x1, blocking collectives, local(): lax.all_to_all(jnp.stack(jnp.split(query_parts.astype(jnp.bfloat16), lax....  38.5 us
    all_gather x1, waiting for transfers between devices, local(): lax.all_gather(queries, 'sp', axis=0, tiled=True)  17 us
    all_gather x1, waiting for transfers between devices, local(): query_all_heads = lax.all_gather(query_grad, 'tp', axis=1, tiled=True)  9.8 us
  transfers between devices with their start and end apart: 6, of which 5 were waited for; matrix products, arithmetic and copies ran while one was open for 10% of the time, Pallas kernels for 0%

profile of v1, /device:TPU:0, one launch (start us, length us, event | category | flops | bytes accessed | tf_op | source)
XLA Modules:
  0.0 394.8 jit_solution(2137687668849269552)
XLA Ops:
  8.8 1.1 convert_multiply_fusion.2
  10.4 32.5 %all_gather.33 = f32[8,1024,4]{1,2,0:T(4,128)S(1)} all-gather(f32[1,1024,4]{1,2,0:T(4,128)S(1)} %constant_dynamic-update-slice_fusion), channel_id=1, replica_groups=mesh['sp'=8,'tp'=4] {'sp'}, dimensions={0}, use_global_device_ids=true | all-gather | bytes 147456 | tf_op jit(solution)/shard_map/all_gather | solution.py:15
  43.6 1.8 constant_dynamic-slice_fusion.1
  45.4 17.0 %all-gather.6.cloned.1.call-done = bf16[1024,1024]{1,0:T(8,128)(2,1)} async-done(((bf16[128,1024]{1,0:T(8,128)(2,1)}), bf16[1024,1024]{1,0:T(8,128)(2,1)}) %all-gather.6.cloned.1.call-update) | async-done | bytes 2097168 | tf_op jit(solution)/shard_map/all_gather | solution.py:52
  62.4 4.5 %reshape.72 = bf16[2,512,4,256]{3,2,1,0:T(4,128)(2,1)} reshape(bf16[1024,1024]{1,0:T(8,128)(2,1)} %all-gather.6.cloned.1.call-done) | data formatting | bytes 4194304 | tf_op jit(solution)/shard_map/reshape | solution.py:57
  66.9 1.9 copy.44
  68.7 3.0 while.46
  68.8 0.8 bitcast_reduce_fusion.2
  69.5 0.7 fusion.69
  70.3 0.8 bitcast_reduce_fusion.2
  71.0 0.7 fusion.69
  71.8 31.3 %all-gather.1 = f32[16,4,512]{2,1,0:T(4,128)S(1)} all-gather(f32[2,4,512]{2,1,0:T(4,128)S(1)} %get-tuple-element.265), channel_id=3, replica_groups=mesh['sp'=8,'tp'=4] {'sp'}, dimensions={0}, use_global_device_ids=true | all-gather | bytes 147456 | tf_op jit(solution)/shard_map/all_gather | solution.py:15
  103.0 30.6 %all-gather = f32[16,4,512]{2,1,0:T(4,128)S(1)} all-gather(f32[2,4,512]{2,1,0:T(4,128)S(1)} %get-tuple-element.264), channel_id=2, replica_groups=mesh['sp'=8,'tp'=4] {'sp'}, dimensions={0}, use_global_device_ids=true | all-gather | bytes 147456 | tf_op jit(solution)/shard_map/all_gather | solution.py:15
  134.3 10.6 %while.47 = (s32[]{:T(128)}, f32[2,4,512]{2,1,0:T(4,128)S(1)}, f32[2,4,512]{2,1,0:T(4,128)S(1)}, f32[1024,4]{0,1:T(4,128)S(1)}, f32[8,2,4,512]{3,2,1,0:T(4,128)}...) while((s32[]{:T(128)}, f32[2,4,512]{2,1,0:T(4,128)S(1)}, ...), condition=%wide.region_6.7_spmd, body=%wide.region_5.6_spmd.sunk | while | flops 28677 | bytes 147599 | solution.py:20
  134.3 0.7 bitcast_add_fusion.2
  135.0 0.8 fusion.70
  135.8 0.7 bitcast_add_fusion.2
  136.6 0.8 fusion.70
  137.3 0.7 bitcast_add_fusion.2
  138.1 0.8 fusion.70
  138.9 0.7 bitcast_add_fusion.2
  139.6 0.8 fusion.70
  140.4 0.7 bitcast_add_fusion.2
  141.1 0.8 fusion.70
  141.9 0.7 bitcast_add_fusion.2
  142.6 0.8 fusion.70
  143.4 0.7 bitcast_add_fusion.2
  144.1 0.8 fusion.70
  145.0 4.5 %reshape.73 = bf16[2,512,4,256]{3,2,1,0:T(4,128)(2,1)} reshape(bf16[1024,1024]{1,0:T(8,128)(2,1)} %all-gather.8.cloned.1.call-done) | data formatting | bytes 4194304 | tf_op jit(solution)/shard_map/reshape | solution.py:58
  149.5 18.0 %while.48 = (s32[]{:T(128)}, f32[512,256]{1,0:T(8,128)S(1)}, f32[512,256]{1,0:T(8,128)S(1)}, bf16[2,512,4,256]{3,1,2,0:T(8,128)(2,1)}, bf16[2,512,4,256]{3,1,2,0...) while((s32[]{:T(128)}, f32[512,256]{1,0:T(8,128)S(1)}, ...), condition=%wide.region_8.9_spmd.clone, body=%wide.region_7.8_spmd.clone.sunk | while | flops 2694316032 | bytes 48029940 | solution.py:102
  149.5 1.6 constant_dynamic-slice_fusion.4
  151.1 0.7 fusion.79
  151.8 1.5 fusion.82
  153.3 1.5 fusion.80
  154.9 0.8 fusion.81
  155.7 0.7 copy-done.1
  157.2 1.3 copy-done.2
  158.5 1.6 constant_dynamic-slice_fusion.4
  160.1 0.7 fusion.79
  160.8 1.5 fusion.82
  162.3 1.6 fusion.80
  163.9 0.9 fusion.81
  164.7 0.7 copy-done.1
  166.2 1.3 copy-done.2
  167.5 4.5 %copy.46 = bf16[2,512,4,256]{3,2,1,0:T(4,128)(2,1)} copy(bf16[2,512,4,256]{3,1,2,0:T(8,128)(2,1)} %get-tuple-element.269) | data formatting | bytes 4194304 | tf_op jit(solution)/shard_map/convert_element_type | solution.py:109
  172.0 3.2 convert_element_type.76
  175.5 38.5 %all_to_all.23 = bf16[8,128,1,1024]{3,1,2,0:T(8,128)(2,1)S(1)} all-to-all(bf16[8,128,1,1024]{3,1,2,0:T(8,128)(2,1)S(1)} %fusion.40), channel_id=1, replica_groups=mesh['sp'=8,'tp'=4] {'sp'}, dimensions={0} | all-to-all | bytes 4194304 | tf_op jit(solution)/shard_map/all_to_all | solution.py:107
  214.0 1.1 reduce_sum.48
  215.3 5.8 %psum.7 = f32[128]{0:T(128)S(1)} all-reduce(f32[128]{0:T(128)S(1)} %fusion.36), channel_id=1, replica_groups=mesh['sp'=8,'tp'=4] {'tp'}, use_global_device_ids=true, to_apply=%region_11.12 | all-reduce | flops 128 | bytes 1024 | tf_op jit(solution)/shard_map/psum | solution.py:146
  221.2 9.8 %all-gather.10.cloned.1.call-done = bf16[128,4096]{1,0:T(8,128)(2,1)} async-done(((bf16[128,1024]{1,0:T(8,128)(2,1)}), bf16[128,4096]{1,0:T(8,128)(2,1)}) %all-gather.10.cloned.1.call-update) | async-done | bytes 1048592 | tf_op jit(solution)/shard_map/all_gather | solution.py:141
  231.0 6.9 %convolution_convert_fusion = bf16[1024,4096]{1,0:T(8,128)(2,1)} fusion(bf16[128,4096]{1,0:T(8,128)(2,1)} %all-gather.10.cloned.1.call-done, bf16[128,1024]{1,0:T(8,128)(2,1)S(1)} %copy-done.3, f32[1024]{0:T(1024)S(1)} %copy-done.8, f32[128]{0:T(128)S(1)} %add_rsqrt_fusion), kind=kOutput, calls=%fused_computation.47 | convolution fusion | flops 1078460416 | bytes 9703936 | tf_op jit(solution)/shard_map/dot_general | solution.py:150
  238.5 0.8 reduce.3
  239.3 0.8 reshape.100
  240.1 3.4 all-to-all-start.1
  243.5 0.8 reduce.4
  244.3 0.8 reshape.102
  245.1 4.4 %all-to-all-done.1 = bf16[4,2,16384]{2,1,0:T(2,128)(2,1)S(1)} async-done(((bf16[4,2,16384]{2,1,0:T(2,128)(2,1)}), bf16[4,2,16384]{2,1,0:T(2,128)(2,1)S(1)}, u32[]{:S(2)}, u32[]{:S(2)}) %all-to-all-start.1) | async-done | bytes 262176 | tf_op jit(solution)/shard_map/all_to_all | solution.py:121
  249.4 3.4 all-to-all-start.2
  254.0 0.9 copy.54
  254.9 3.9 all-to-all-done.2
  260.0 0.9 copy.55
  260.9 7.0 %convolution_convert_fusion.1 = bf16[128,1024]{1,0:T(8,128)(2,1)} fusion(bf16[128,4096]{1,0:T(8,128)(2,1)S(1)} %copy-done, bf16[1024,4096]{1,0:T(8,128)(2,1)} %param.16), kind=kOutput, calls=%fused_computation.48 | convolution fusion | flops 1073872896 | bytes 9699328 | tf_op jit(solution)/shard_map/dot_general | solution.py:142
  267.9 117.6 %reduce-scatter.2.cloned.1.call-done = bf16[128,4096]{1,0:T(8,128)(2,1)} async-done(((bf16[1024,4096]{1,0:T(8,128)(2,1)}), bf16[128,4096]{1,0:T(8,128)(2,1)}) %reduce-scatter.2.cloned.1.call-update) | async-done | bytes 1048592 | tf_op jit(solution)/shard_map/reduce_scatter | solution.py:149
  385.6 2.8 convert_element_type.81
  (70 shorter events, 8.1 us)
Async XLA Ops:
  7.2 55.2 %all-gather.6.cloned.1.call-start = ((), (), s32[]{:S(2)}) async-start(), calls=%async_computation.4 | async-start | bytes 2359296 | tf_op jit(solution)/shard_map/all_gather | solution.py:52
  7.9 137.1 %all-gather.8.cloned.1.call-start = ((), (), s32[]{:S(2)}) async-start(), calls=%async_computation.5 | async-start | bytes 2359296 | tf_op jit(solution)/shard_map/all_gather | solution.py:53
  8.6 222.4 %all-gather.10.cloned.1.call-start = ((), (), s32[]{:S(2)}) async-start(), calls=%async_computation.6 | async-start | bytes 1310720 | tf_op jit(solution)/shard_map/all_gather | solution.py:141
  42.9 0.7 copy-start.4
  103.0 30.6 %copy-start.5 = (f32[16,4,512]{2,1,0:T(4,128)}, f32[16,4,512]{2,1,0:T(4,128)S(1)}, u32[]{:S(2)}) copy-start(f32[16,4,512]{2,1,0:T(4,128)S(1)} %all-gather.1) | copy-start | bytes 393220
  133.7 0.7 copy-start.6
  151.8 1.5 copy-start.7
  154.9 1.6 copy-start.1
  157.2 1.3 copy-start.2
  160.8 1.5 copy-start.7
  163.9 1.6 copy-start.1
  166.2 1.3 copy-start.2
  214.0 1.2 copy-start.3
  214.0 17.0 %copy-start.8 = (f32[1024]{0:T(1024)S(1)}, f32[1024]{0:T(1024)}, u32[]{:S(2)}) copy-start(f32[1024]{0:T(1024)} %param.15) | copy-start | bytes 12292
  215.2 170.4 %reduce-scatter.2.cloned.1.call-start = ((), (), s32[]{:S(2)}) async-start(), calls=%async_computation.7 | async-start | bytes 9437184 | tf_op jit(solution)/shard_map/reduce_scatter | solution.py:149
  240.1 9.4 %all-to-all-start.1 = ((bf16[4,2,16384]{2,1,0:T(2,128)(2,1)}), bf16[4,2,16384]{2,1,0:T(2,128)(2,1)S(1)}, u32[]{:S(2)}, u32[]{:S(2)}) async-start(bf16[4,2,16384]{2,1,0:T(2,128)(2,1)} %reshape.100), calls=%async_computation.2 | async-start | bytes 524288 | tf_op jit(solution)/shard_map/all_to_all | solution.py:121
  249.4 9.4 %all-to-all-start.2 = ((bf16[4,2,16384]{2,1,0:T(2,128)(2,1)}), bf16[4,2,16384]{2,1,0:T(2,128)(2,1)S(1)}, u32[]{:S(2)}, u32[]{:S(2)}) async-start(bf16[4,2,16384]{2,1,0:T(2,128)(2,1)} %reshape.102), calls=%async_computation.3 | async-start | bytes 524288 | tf_op jit(solution)/shard_map/all_to_all | solution.py:124
  254.9 6.0 %copy-start = (bf16[128,4096]{1,0:T(8,128)(2,1)S(1)}, bf16[128,4096]{1,0:T(8,128)(2,1)}, u32[]{:S(2)}) copy-start(bf16[128,4096]{1,0:T(8,128)(2,1)} %all-gather.10.cloned.1.call-done) | copy-start | bytes 3145732
Sparse Core Ops, SparseCore 0:
  10.1 52.2 all-gather.5
  64.5 49.3 all-gather.7
  215.3 15.6 all-gather.9
  238.0 147.4 reduce-scatter.1
